TPU v7x, 32 devices: a whole 2x2x4 slice. The times are simulated.
32 devices in a mesh: sp: 16 (over z, y, x), tp: 2 (over core).
Axes of the slice: x: 2, y: 2, z: 4, core: 2. Of those that a mesh axis runs over, the one named last changes fastest.
Arguments:
- tokens: bfloat16 [4096, 2048], P('sp', 'tp'), may hold values from -6 to 6
- norm_gain: float32 [2048], replicated, may hold values from 0.1 to 1.9
- query_weight: bfloat16 [1024, 2048], P('tp'), may hold values from -0.125 to 0.125
- key_weight: bfloat16 [1024, 2048], P('tp'), may hold values from -0.125 to 0.125
- value_weight: bfloat16 [1024, 2048], P('tp'), may hold values from -0.125 to 0.125
- pool_weight: bfloat16 [1024, 2048], P('tp'), may hold values from -0.125 to 0.125
- query_gain: float32 [64], replicated, may hold values from 0.6 to 6
- key_gain: float32 [64], replicated, may hold values from 0.6 to 6
- cum_gate: float32 [4096, 16], P('sp', 'tp'), as said below
- out_pool_weight: bfloat16 [1024, 2048], P(None, 'tp'), may hold values from -0.1875 to 0.1875
- out_attn_weight: bfloat16 [1024, 2048], P(None, 'tp'), may hold values from -0.1875 to 0.1875
Outputs:
- mixed: bfloat16 [4096, 2048], P('sp', 'tp')
Inputs may be any that keep to these rules, and one draw needn't show every extreme that they name: `cum_gate`: in each head the values never rise along the positions.
All inputs are finite; a program needn't handle non-finite values.
Results may differ from a plain program's by a relative error of at most 0.005.
The roundings to bfloat16 on the way count: a program that leaves them out, or rounds other values in their place, can miss the bound.
Values may be sent and summed in bfloat16 or wider, within the bound.
A program may use at most 128 MiB of HBM per device.

v0:
```python
import math
import jax
import jax.numpy as jnp
from jax import lax
from jax.sharding import PartitionSpec as P

HEAD_DIM = 64
POOL_WIDTH = 1024
POOL_GROUPS = 4
epsilon = 1e-06
masked_fill = -1e30


def from_behind(value, axis, steps):
    count = lax.axis_size(axis)
    leading, last = (max(0, -steps), min(count, count - steps))
    return lax.ppermute(value, axis, [(source, source + steps) for source in range(leading, last)])


def rms_scale(values, gain):
    return values * lax.rsqrt(jnp.mean(values * values, axis=-1, keepdims=True) + epsilon) * gain


def block_partials(query_rows, query_pos, query_gate, key_rows, value_rows, key_pos, key_gate):
    logits = jnp.einsum("qhd,gkhd->qhgk", query_rows, key_rows, preferred_element_type=jnp.float32)
    logits = logits + query_gate[:, :, None, None] - jnp.transpose(key_gate, (2, 0, 1))[None]
    allowed = key_pos[None, None, :, :] <= query_pos[:, None, None, None]
    logits = jnp.where(allowed, logits, masked_fill)
    block_max = jnp.max(logits, axis=-1)
    weights = jnp.where(allowed, jnp.exp(logits - block_max[..., None]), 0.0)
    totals = jnp.sum(weights, axis=-1)
    numerator = jnp.einsum(
        "qhgk,gkhd->qhgd",
        weights.astype(jnp.bfloat16),
        value_rows,
        preferred_element_type=jnp.float32,
    )
    return (block_max, totals, numerator)


def merge_state(state, partials):
    run_max, run_den, run_acc = state
    block_max, totals, numerator = partials
    new_max = jnp.maximum(run_max, jnp.max(block_max, axis=-1))
    old_scale = jnp.exp(run_max - new_max)
    block_scale = jnp.exp(block_max - new_max[..., None])
    new_den = run_den * old_scale + jnp.sum(block_scale * totals, axis=-1)
    new_acc = run_acc * old_scale[..., None] + jnp.sum(block_scale[..., None] * numerator, axis=2)
    return (new_max, new_den, new_acc)


def empty_state(rows, heads_here):
    return (
        jnp.full((rows, heads_here), masked_fill, jnp.float32),
        jnp.zeros((rows, heads_here), jnp.float32),
        jnp.zeros((rows, heads_here, HEAD_DIM), jnp.float32),
    )


def per_device(
    tokens,
    norm_gain,
    query_weight,
    key_weight,
    value_weight,
    pool_weight,
    query_gain,
    key_gain,
    cum_gate,
    out_pool_weight,
    out_attn_weight,
):
    full_rows = lax.all_gather(tokens, "tp", axis=1, tiled=True)
    normed = rms_scale(full_rows.astype(jnp.float32), norm_gain).astype(jnp.bfloat16)
    length = full_rows.shape[0]
    heads_here = cum_gate.shape[1]
    offset = lax.axis_index("sp") * length

    def project(weight):
        return lax.dot_general(
            normed, weight, (((1,), (1,)), ((), ())), preferred_element_type=jnp.float32
        )

    query_heads = (
        rms_scale(project(query_weight).reshape(length, heads_here, HEAD_DIM), query_gain)
        * HEAD_DIM ** (-0.5)
    ).astype(jnp.bfloat16)
    key_heads = rms_scale(
        project(key_weight).reshape(length, heads_here, HEAD_DIM), key_gain
    ).astype(jnp.bfloat16)
    value_heads = project(value_weight).astype(jnp.bfloat16).reshape(length, heads_here, HEAD_DIM)
    pool_input = project(pool_weight).astype(jnp.bfloat16)
    reach = 2**POOL_GROUPS
    rim_rows = from_behind(pool_input[length - reach :], "sp", 1)
    extended = jnp.concatenate([rim_rows, pool_input], axis=0).astype(jnp.float32)
    prefix = jnp.cumsum(extended, axis=0)
    width_here = pool_input.shape[1]
    channel_ids = lax.axis_index("tp") * width_here + jnp.arange(width_here, dtype=jnp.int32)
    group_ids = channel_ids // (POOL_WIDTH // POOL_GROUPS)
    counts = (offset + jnp.arange(1, length + 1, dtype=jnp.int32)).astype(jnp.float32)[:, None]
    current = prefix[reach:]
    pooled_mean = jnp.zeros((length, width_here), jnp.float32)
    for group_index in range(POOL_GROUPS):
        window = 2 ** (group_index + 1)
        lagged = prefix[reach - window : reach - window + length]
        average = (current - lagged) / jnp.minimum(counts, float(window))
        pooled_mean = jnp.where(group_ids[None, :] == group_index, average, pooled_mean)
    pooled = (pooled_mean - extended[reach:]).astype(jnp.bfloat16)
    gate_all = lax.all_gather(cum_gate, "sp", axis=0, tiled=True)
    query_pos = offset + jnp.arange(length, dtype=jnp.int32)
    key_flat = key_heads.reshape(length, heads_here * HEAD_DIM)
    value_flat = value_heads.reshape(length, heads_here * HEAD_DIM)

    def absorb(carried, inputs):
        key_rows, value_rows, key_gate, key_pos = inputs
        partials = block_partials(
            query_heads, query_pos, cum_gate, key_rows, value_rows, key_pos, key_gate
        )
        return (merge_state(carried, partials), None)

    key_piece = lax.all_gather(key_flat, "sp", axis=0, tiled=True)
    value_piece = lax.all_gather(value_flat, "sp", axis=0, tiled=True)
    shards = key_piece.shape[0] // length
    grouping = math.gcd(shards, 8)
    turns = shards // grouping
    key_groups = key_piece.reshape(turns, grouping, length, heads_here, HEAD_DIM)
    value_groups = value_piece.reshape(turns, grouping, length, heads_here, HEAD_DIM)
    gate_groups = gate_all.reshape(turns, grouping, length, heads_here)
    pos_groups = jnp.arange(shards * length, dtype=jnp.int32).reshape(turns, grouping, length)
    result, _ = lax.scan(
        absorb, empty_state(length, heads_here), (key_groups, value_groups, gate_groups, pos_groups)
    )
    final_max, final_den, final_acc = result
    attended = (
        (final_acc / final_den[..., None])
        .reshape(length, heads_here * HEAD_DIM)
        .astype(jnp.bfloat16)
    )
    pool_full, attn_full = (
        lax.all_gather(pooled, "tp", axis=1, tiled=True),
        lax.all_gather(attended, "tp", axis=1, tiled=True),
    )
    output = jnp.dot(pool_full, out_pool_weight, preferred_element_type=jnp.float32) + jnp.dot(
        attn_full, out_attn_weight, preferred_element_type=jnp.float32
    )
    return output.astype(jnp.bfloat16)


def solution(mesh):
    return jax.shard_map(
        per_device,
        mesh=mesh,
        in_specs=(
            P("sp", "tp"),
            P(),
            P("tp", None),
            P("tp", None),
            P("tp", None),
            P("tp", None),
            P(),
            P(),
            P("sp", "tp"),
            P(None, "tp"),
            P(None, "tp"),
        ),
        out_specs=P("sp", "tp"),
        check_vma=False,
    )
```

profile of v0, /device:TPU:0, one launch (start us, length us, event | category | flops | bytes accessed | tf_op | source)
XLA Modules:
  0.0 260.2 jit_solution(4839599759511507353)
XLA Ops:
  8.0 12.6 %all-gather.4.cloned.1.call-done = bf16[256,2048]{1,0:T(8,128)(2,1)} async-done(((bf16[256,1024]{1,0:T(8,128)(2,1)}), bf16[256,2048]{1,0:T(8,128)(2,1)}) %all-gather.4.cloned.1.call-update) | async-done | bytes 1048592 | tf_op jit(solution)/shard_map/all_gather | solution.py:73
  20.7 1.5 fusion.24
  22.2 2.8 %fusion.50 = (f32[256,512]{1,0:T(8,128)S(1)}, f32[256,512]{1,0:T(8,128)}) fusion(bf16[512,2048]{1,0:T(8,128)(2,1)S(1)} %copy-done, bf16[256,2048]{1,0:T(8,128)(2,1)} %all-gather.4.cloned.1.call-done, f32[2048]{0:T(1024)} %param.14, f32[256]{0:T(256)S(1)} %add_rsqrt_fusion.2), kind=kOutput, calls=%fused_computation.93 | convolution fusion | flops 539099136 | bytes 4203520 | tf_op jit(solution)/shard_map/dot_general | solution.py:80
  26.9 3.0 %convolution_convert_fusion = bf16[256,512]{1,0:T(8,128)(2,1)} fusion(bf16[512,2048]{1,0:T(8,128)(2,1)} %param.17, bf16[256,2048]{1,0:T(8,128)(2,1)S(1)} %copy-done.4, f32[2048]{0:T(1024)S(1)} %copy-done.9, f32[256]{0:T(256)S(1)} %add_rsqrt_fusion.2), kind=kOutput, calls=%fused_computation.41 | convolution fusion | flops 539099136 | bytes 3417088 | tf_op jit(solution)/shard_map/dot_general | solution.py:80
  30.0 42.8 %all_gather.21 = f32[4096,8]{0,1:T(8,128)S(1)} all-gather(f32[256,8]{0,1:T(8,128)S(1)} %copy-done.6), channel_id=1, replica_groups=mesh['sp'=16,'tp'=2] {'sp'}, dimensions={0}, use_global_device_ids=true | all-gather | bytes 139264 | tf_op jit(solution)/shard_map/all_gather | solution.py:109
  72.9 2.5 convolution_convert_fusion.1
  75.4 1.3 collective-permute-start
  80.2 2.5 all_gather.19
  83.4 20.9 %all-gather.6.cloned.1.call-done = bf16[4096,512]{1,0:T(8,128)(2,1)} async-done(((bf16[256,512]{1,0:T(8,128)(2,1)}), bf16[4096,512]{1,0:T(8,128)(2,1)}) %all-gather.6.cloned.1.call-update) | async-done | bytes 4194320 | tf_op jit(solution)/shard_map/all_gather | solution.py:121
  104.3 11.2 %reshape.154 = bf16[2,8,256,8,64]{4,3,2,1,0:T(8,128)(2,1)} reshape(bf16[4096,512]{1,0:T(8,128)(2,1)} %all-gather.6.cloned.1.call-done) | data formatting | bytes 8388608 | tf_op jit(solution)/shard_map/reshape | solution.py:126
  115.5 9.8 %copy.42 = bf16[2,8,256,8,64]{2,4,1,3,0:T(8,128)(2,1)} copy(bf16[2,8,256,8,64]{4,3,2,1,0:T(8,128)(2,1)} %reshape.154) | data formatting | bytes 8388608
  125.3 56.0 %all-gather.8.cloned.1.call-done = bf16[4096,512]{1,0:T(8,128)(2,1)} async-done(((bf16[256,512]{1,0:T(8,128)(2,1)}), bf16[4096,512]{1,0:T(8,128)(2,1)}) %all-gather.8.cloned.1.call-update) | async-done | bytes 4194320 | tf_op jit(solution)/shard_map/all_gather | solution.py:122
  181.3 11.2 %reshape.155 = bf16[2,8,256,8,64]{4,3,2,1,0:T(8,128)(2,1)} reshape(bf16[4096,512]{1,0:T(8,128)(2,1)} %all-gather.8.cloned.1.call-done) | data formatting | bytes 8388608 | tf_op jit(solution)/shard_map/reshape | solution.py:127
  192.5 9.8 %copy.44 = bf16[2,8,256,8,64]{2,4,1,3,0:T(8,128)(2,1)} copy(bf16[2,8,256,8,64]{4,3,2,1,0:T(8,128)(2,1)} %reshape.155) | data formatting | bytes 8388608
  202.2 46.0 %while.15 = (s32[]{:T(128)}, f32[256,8]{0,1:T(8,128)S(1)}, f32[256,8]{0,1:T(8,128)S(1)}, f32[256,8,64]{0,2,1:T(8,128)S(1)}, s32[2,8,256]{2,1,0:T(8,128)S(1)}, /*...) while((s32[]{:T(128)}, f32[256,8]{0,1:T(8,128)S(1)}, ...), condition=%wide.region_11.12_spmd.clone, body=%wide.region_5.11_spmd.clone.sunk | while | flops 1122789632 | bytes 127101120 | solution.py:130
  202.8 6.9 %fusion.69 = (f32[256,8,8]{0,2,1:T(8,128)S(1)}, f32[256,8,8,256]{0,3,2,1:T(8,128)S(1)}) fusion(f32[8,8,256]{2,1,0:T(8,128)S(1)} %bitcast.72, f32[256,8]{0,1:T(8,128)S(1)} %get-tuple-element.297, bf16[256,8,64]{0,2,1:T(8,128)(2,1)S(1)} %get-tuple-element.296, bf16[2,8,256,8,64]{2,4,1,3,0:T(8,128)(2,1)} %get-tuple-element.295, s32[]{:T(128)S(6)} %copy.63, ...), kind=kOutput, calls=%fused_computation.92.clone.1 | convolution fusion | flops 553631744 | bytes 19800068 | tf_op jit(solution)/shard_map/while/body/eval_jaxpr/qhd,gkhd->qhgk/dot_general | solution.py:25
  209.7 4.8 %fusion.70 = (f32[256,8,8]{0,2,1:T(8,128)S(1)}, f32[256,8]{0,1:T(8,128)S(1)}) fusion(f32[256,8,8,256]{0,3,2,1:T(8,128)S(1)} %get-tuple-element.256, f32[256,8,8]{0,2,1:T(8,128)S(1)} %get-tuple-element.257, pred[256,8,256]{0,2,1:T(8,128)(4,1)S(1)} %broadcast_compare_fusion.6), kind=kLoop, calls=%fused_computation.6.clone.1 | loop fusion | flops 16758784 | bytes 17440768 | tf_op jit(solution)/shard_map/while/body/eval_jaxpr/reduce_sum | solution.py:31
  214.5 0.9 copy-done.2
  215.5 9.5 %fusion.72 = f32[256,8,64]{0,2,1:T(8,128)S(1)} fusion(f32[256,8,8,256]{0,3,2,1:T(8,128)} %copy-done.2, f32[256,8,8]{0,2,1:T(8,128)S(1)} %get-tuple-element.257, pred[256,8,256]{0,2,1:T(8,128)(4,1)S(1)} %broadcast_compare_fusion.6, bf16[2,8,256,8,64]{2,4,1,3,0:T(8,128)(2,1)} %get-tuple-element.299, s32[]{:T(128)S(6)} %copy.63, ...), kind=kOutput, calls=%fused_computation.12.clone.1 | convolution fusion | flops 551419904 | bytes 20054020 | tf_op jit(solution)/shard_map/while/body/eval_jaxpr/qhgk,gkhd->qhgd/dot_general | solution.py:32
  225.8 6.9 %fusion.69 = (f32[256,8,8]{0,2,1:T(8,128)S(1)}, f32[256,8,8,256]{0,3,2,1:T(8,128)S(1)}) fusion(f32[8,8,256]{2,1,0:T(8,128)S(1)} %bitcast.72, f32[256,8]{0,1:T(8,128)S(1)} %get-tuple-element.297, bf16[256,8,64]{0,2,1:T(8,128)(2,1)S(1)} %get-tuple-element.296, bf16[2,8,256,8,64]{2,4,1,3,0:T(8,128)(2,1)} %get-tuple-element.295, s32[]{:T(128)S(6)} %copy.63, ...), kind=kOutput, calls=%fused_computation.92.clone.1 | convolution fusion | flops 553631744 | bytes 19800068 | tf_op jit(solution)/shard_map/while/body/eval_jaxpr/qhd,gkhd->qhgk/dot_general | solution.py:25
  232.7 4.8 %fusion.70 = (f32[256,8,8]{0,2,1:T(8,128)S(1)}, f32[256,8]{0,1:T(8,128)S(1)}) fusion(f32[256,8,8,256]{0,3,2,1:T(8,128)S(1)} %get-tuple-element.256, f32[256,8,8]{0,2,1:T(8,128)S(1)} %get-tuple-element.257, pred[256,8,256]{0,2,1:T(8,128)(4,1)S(1)} %broadcast_compare_fusion.6), kind=kLoop, calls=%fused_computation.6.clone.1 | loop fusion | flops 16758784 | bytes 17440768 | tf_op jit(solution)/shard_map/while/body/eval_jaxpr/reduce_sum | solution.py:31
  238.5 9.5 %fusion.72 = f32[256,8,64]{0,2,1:T(8,128)S(1)} fusion(f32[256,8,8,256]{0,3,2,1:T(8,128)} %copy-done.2, f32[256,8,8]{0,2,1:T(8,128)S(1)} %get-tuple-element.257, pred[256,8,256]{0,2,1:T(8,128)(4,1)S(1)} %broadcast_compare_fusion.6, bf16[2,8,256,8,64]{2,4,1,3,0:T(8,128)(2,1)} %get-tuple-element.299, s32[]{:T(128)S(6)} %copy.63, ...), kind=kOutput, calls=%fused_computation.12.clone.1 | convolution fusion | flops 551419904 | bytes 20054020 | tf_op jit(solution)/shard_map/while/body/eval_jaxpr/qhgk,gkhd->qhgd/dot_general | solution.py:32
  248.3 2.3 all_gather.23
  250.6 3.1 %fusion.27 = bf16[256,1024]{1,0:T(8,128)(2,1)} fusion(f32[256,1024]{1,0:T(8,128)S(1)} %fusion.51, bf16[256,1024]{0,1:T(8,128)(2,1)S(1)} %all_gather.23, bf16[1024,1024]{1,0:T(8,128)(2,1)} %param.23), kind=kOutput, calls=%fused_computation.40 | convolution fusion | flops 537395200 | bytes 4194304 | tf_op jit(solution)/shard_map/dot_general | solution.py:143
  (79 shorter events, 10.0 us)
Async XLA Ops:
  6.5 15.6 %copy-start = (bf16[512,2048]{1,0:T(8,128)(2,1)S(1)}, bf16[512,2048]{1,0:T(8,128)(2,1)}, u32[]{:S(2)}) copy-start(bf16[512,2048]{1,0:T(8,128)(2,1)} %param.16) | copy-start | bytes 6291460
  6.5 14.1 %all-gather.4.cloned.1.call-start = ((), (), s32[]{:S(2)}) async-start(), calls=%async_computation | async-start | bytes 1572864 | tf_op jit(solution)/shard_map/all_gather | solution.py:73
  7.3 97.0 %all-gather.6.cloned.1.call-start = ((), (), s32[]{:S(2)}) async-start(), calls=%async_computation.1 | async-start | bytes 4456448 | tf_op jit(solution)/shard_map/all_gather | solution.py:121
  25.0 1.0 copy-start.5
  25.2 1.7 copy-start.4
  25.2 1.7 copy-start.9
  26.8 3.2 %copy-start.6 = (f32[256,8]{0,1:T(8,128)S(1)}, f32[256,8]{0,1:T(8,128)}, u32[]{:S(2)}) copy-start(f32[256,8]{0,1:T(8,128)} %param.21) | copy-start | bytes 24580
  26.9 154.4 %all-gather.8.cloned.1.call-start = ((), (), s32[]{:S(2)}) async-start(), calls=%async_computation.2 | async-start | bytes 4456448 | tf_op jit(solution)/shard_map/all_gather | solution.py:122
  72.9 3.8 %copy-start.8 = (bf16[512,2048]{1,0:T(8,128)(2,1)S(1)}, bf16[512,2048]{1,0:T(8,128)(2,1)}, u32[]{:S(2)}) copy-start(bf16[512,2048]{1,0:T(8,128)(2,1)} %param.15) | copy-start | bytes 6291460
  75.4 2.2 copy-start.7
  75.4 3.0 %collective-permute-start = (bf16[16,512]{1,0:T(8,128)(2,1)S(1)}, bf16[16,512]{1,0:T(8,128)(2,1)S(1)}, u32[]{:S(2)}, u32[]{:S(2)}) collective-permute-start(bf16[16,512]{1,0:T(8,128)(2,1)S(1)} %slice.42), channel_id=1, source_target_pairs={{0,2},{2,4},{4,6},{6,8},{8,10},{10,12},{12,14},{14,16},{16,18},{18... | collective-permute-start | bytes 49160 | tf_op jit(solution)/shard_map/ppermute | solution.py:17
  79.7 3.0 %copy-start.3 = (bf16[1024,1024]{1,0:T(8,128)(2,1)S(1)}, bf16[1024,1024]{1,0:T(8,128)(2,1)}, u32[]{:S(2)}) copy-start(bf16[1024,1024]{1,0:T(8,128)(2,1)} %param.22) | copy-start | bytes 6291460
  209.7 5.7 %copy-start.2 = (f32[256,8,8,256]{0,3,2,1:T(8,128)}, f32[256,8,8,256]{0,3,2,1:T(8,128)S(1)}, u32[]{:S(2)}) copy-start(f32[256,8,8,256]{0,3,2,1:T(8,128)S(1)} %get-tuple-element.256) | copy-start | bytes 50331652 | tf_op jit(solution)/shard_map/while
  232.7 5.7 %copy-start.2 = (f32[256,8,8,256]{0,3,2,1:T(8,128)}, f32[256,8,8,256]{0,3,2,1:T(8,128)S(1)}, u32[]{:S(2)}) copy-start(f32[256,8,8,256]{0,3,2,1:T(8,128)S(1)} %get-tuple-element.256) | copy-start | bytes 50331652 | tf_op jit(solution)/shard_map/while
  248.2 5.4 %copy-start.1 = (bf16[512,2048]{1,0:T(8,128)(2,1)S(1)}, bf16[512,2048]{1,0:T(8,128)(2,1)}, u32[]{:S(2)}) copy-start(bf16[512,2048]{1,0:T(8,128)(2,1)} %param.16) | copy-start | bytes 6291460
Sparse Core Ops, SparseCore 0:
  8.9 11.7 all-gather.3
  27.0 77.2 all-gather.5
  107.1 74.1 all-gather.7
where the time goes:
time: 262 us; the launch traced here: 260 us
  waiting for transfers between devices  90.9 us (35%)
  blocking collectives  47.6 us (18%)
  local copies, waits for them, and re-layouts  45.9 us (18%)
  matrix products  45.8 us (17%)
  other arithmetic  15 us (6%)
  between operations  13.4 us (5%)
    all_gather x1, waiting for transfers between devices, per_device(): value_piece = lax.all_gather(value_flat, 'sp', axis=0, tiled=True)  56 us
    all_gather x1, blocking collectives, per_device(): gate_all = lax.all_gather(cum_gate, 'sp', axis=0, tiled=True)  42.8 us
    all_gather x1, waiting for transfers between devices, per_device(): key_piece = lax.all_gather(key_flat, 'sp', axis=0, tiled=True)  20.9 us
    unnamed x20, local copies, waits for them, and re-layouts  20.1 us
    dot_general x2, matrix products, block_partials(): jnp.einsum('qhgk,gkhd->qhgd', weights.astype(jnp.bfloat16), value_rows, p...  19 us
    dot_general x2, matrix products, block_partials(): jnp.einsum('qhd,gkhd->qhgk', query_rows, key_rows, preferred_element_type...  13.8 us
    all_gather x1, waiting for transfers between devices, per_device(): full_rows = lax.all_gather(tokens, 'tp', axis=1, tiled=True)  12.6 us
    reshape x1, local copies, waits for them, and re-layouts, per_device(): key_piece.reshape(turns, grouping, length, heads_here, HEAD_DIM)  11.2 us
  transfers between devices with their start and end apart: 4, of which 4 were waited for; matrix products, arithmetic and copies ran while one was open for 12% of the time, Pallas kernels for 0%

commit v1 on v0

--- a/solution.py
+++ b/solution.py
@@ -119,7 +119,15 @@
         return (merge_state(carried, partials), None)
 
     key_piece = lax.all_gather(key_flat, "sp", axis=0, tiled=True)
-    value_piece = lax.all_gather(value_flat, "sp", axis=0, tiled=True)
+    found = [value_flat]
+    n_slots = lax.psum(1, "sp")
+    s = 0
+    while s < n_slots - 1:
+        ready = lax.ppermute(found[-1], "sp", [(ii, (ii + 1) % n_slots) for ii in range(n_slots)])
+        found.append(ready)
+        s += 1
+    current_block = jnp.concatenate(found[::-1], 0)
+    value_piece = jnp.roll(current_block, (lax.axis_index("sp") + 1) * value_flat.shape[0], axis=0)
     shards = key_piece.shape[0] // length
     grouping = math.gcd(shards, 8)
     turns = shards // grouping

time: 262 us -> 340 us (1.30)
  waiting for transfers between devices: 90.9 us -> 147 us
  local copies, waits for them, and re-layouts: 45.9 us -> 58.4 us
  matrix products: 45.8 us -> 50.7 us
    ppermute x0 -> x15, waiting for transfers between devices: none -> 133 us  [per_device(): lax.ppermute(found[-1], 'sp', [(ii, (ii + 1) % n_slots) for ii in range(n...]
    all_gather x1 -> x0, waiting for transfers between devices: 56 us -> none  [per_device(): value_piece = lax.all_gather(value_flat, 'sp', axis=0, tiled=True)]
    all_gather x1, waiting for transfers between devices: 20.9 us -> 0.01 us  [per_device(): key_piece = lax.all_gather(key_flat, 'sp', axis=0, tiled=True)]
    unnamed x20 -> x89, local copies, waits for them, and re-layouts: 20.1 us -> 29.3 us
  transfers between devices with their start and end apart: 4 -> 18, of which waited for: 4 -> 15; matrix products, arithmetic and copies ran while one was open for 12% -> 14% of each run, Pallas kernels for 0% -> 0%
where the time goes in v1:
time: 340 us; the launch traced here: 338 us
  waiting for transfers between devices  147 us (43%)
  local copies, waits for them, and re-layouts  58.4 us (17%)
  matrix products  50.7 us (15%)
  blocking collectives  48.2 us (14%)
  other arithmetic  15.8 us (5%)
  between operations  14.1 us (4%)
  starting transfers between devices  3.54 us (1%)
    ppermute x15, waiting for transfers between devices, per_device(): lax.ppermute(found[-1], 'sp', [(ii, (ii + 1) % n_slots) for ii in range(n...  133 us
    all_gather x1, blocking collectives, per_device(): gate_all = lax.all_gather(cum_gate, 'sp', axis=0, tiled=True)  43.5 us
    unnamed x89, local copies, waits for them, and re-layouts  29.3 us
    dot_general x2, matrix products, block_partials(): jnp.einsum('qhgk,gkhd->qhgd', weights.astype(jnp.bfloat16), value_rows, p...  19 us
    dot_general x2, matrix products, block_partials(): jnp.einsum('qhd,gkhd->qhgk', query_rows, key_rows, preferred_element_type...  13.9 us
    all_gather x1, waiting for transfers between devices, per_device(): full_rows = lax.all_gather(tokens, 'tp', axis=1, tiled=True)  13.4 us
    reshape x1, local copies, waits for them, and re-layouts, per_device(): key_piece.reshape(turns, grouping, length, heads_here, HEAD_DIM)  11.2 us
    reshape x1, local copies, waits for them, and re-layouts, per_device(): value_piece.reshape(turns, grouping, length, heads_here, HEAD_DIM)  11.2 us
  transfers between devices with their start and end apart: 18, of which 15 were waited for; matrix products, arithmetic and copies ran while one was open for 14% of the time, Pallas kernels for 0%

profile of v1, /device:TPU:0, one launch (start us, length us, event | category | flops | bytes accessed | tf_op | source)
XLA Modules:
  0.0 338.4 jit_solution(18023697523310996248)
XLA Ops:
  7.3 13.4 %all-gather.3.cloned.1.call-done = bf16[256,2048]{1,0:T(8,128)(2,1)} async-done(((bf16[256,1024]{1,0:T(8,128)(2,1)}), bf16[256,2048]{1,0:T(8,128)(2,1)}) %all-gather.3.cloned.1.call-update) | async-done | bytes 1048592 | tf_op jit(solution)/shard_map/all_gather | solution.py:73
  27.3 10.4 %collective-permute-done.1 = bf16[256,512]{1,0:T(8,128)(2,1)S(1)} collective-permute-done((bf16[256,512]{1,0:T(8,128)(2,1)S(1)}, bf16[256,512]{1,0:T(8,128)(2,1)S(1)}, u32[]{:S(2)}, u32[]{:S(2)}) %collective-permute-start.1) | collective-permute-done | bytes 262176 | tf_op jit(solution)/shard_map/ppermute | solution.py:126
  38.5 11.3 %collective-permute-done.2 = bf16[256,512]{1,0:T(8,128)(2,1)S(1)} collective-permute-done((bf16[256,512]{1,0:T(8,128)(2,1)S(1)}, bf16[256,512]{1,0:T(8,128)(2,1)S(1)}, u32[]{:S(2)}, u32[]{:S(2)}) %collective-permute-start.2) | collective-permute-done | bytes 262176 | tf_op jit(solution)/shard_map/ppermute | solution.py:126
  50.5 9.7 %collective-permute-done.3 = bf16[256,512]{1,0:T(8,128)(2,1)S(1)} collective-permute-done((bf16[256,512]{1,0:T(8,128)(2,1)S(1)}, bf16[256,512]{1,0:T(8,128)(2,1)S(1)}, u32[]{:S(2)}, u32[]{:S(2)}) %collective-permute-start.3) | collective-permute-done | bytes 262176 | tf_op jit(solution)/shard_map/ppermute | solution.py:126
  70.6 9.7 %collective-permute-done.5 = bf16[256,512]{1,0:T(8,128)(2,1)S(1)} collective-permute-done((bf16[256,512]{1,0:T(8,128)(2,1)S(1)}, bf16[256,512]{1,0:T(8,128)(2,1)S(1)}, u32[]{:S(2)}, u32[]{:S(2)}) %collective-permute-start.5) | collective-permute-done | bytes 262176 | tf_op jit(solution)/shard_map/ppermute | solution.py:126
  81.1 9.2 %collective-permute-done.6 = bf16[256,512]{1,0:T(8,128)(2,1)S(1)} collective-permute-done((bf16[256,512]{1,0:T(8,128)(2,1)S(1)}, bf16[256,512]{1,0:T(8,128)(2,1)S(1)}, u32[]{:S(2)}, u32[]{:S(2)}) %collective-permute-start.6) | collective-permute-done | bytes 262176 | tf_op jit(solution)/shard_map/ppermute | solution.py:126
  90.4 16.8 %collective-permute-done.7 = bf16[256,512]{1,0:T(8,128)(2,1)S(1)} collective-permute-done((bf16[256,512]{1,0:T(8,128)(2,1)S(1)}, bf16[256,512]{1,0:T(8,128)(2,1)S(1)}, u32[]{:S(2)}, u32[]{:S(2)}) %collective-permute-start.7) | collective-permute-done | bytes 262176 | tf_op jit(solution)/shard_map/ppermute | solution.py:126
  107.2 43.5 %all_gather.18 = f32[4096,8]{0,1:T(8,128)S(1)} all-gather(f32[256,8]{0,1:T(8,128)S(1)} %copy-done.26), channel_id=1, replica_groups=mesh['sp'=16,'tp'=2] {'sp'}, dimensions={0}, use_global_device_ids=true | all-gather | bytes 139264 | tf_op jit(solution)/shard_map/all_gather | solution.py:109
  155.2 7.6 %collective-permute-done.9 = bf16[256,512]{1,0:T(8,128)(2,1)S(1)} collective-permute-done((bf16[256,512]{1,0:T(8,128)(2,1)S(1)}, bf16[256,512]{1,0:T(8,128)(2,1)S(1)}, u32[]{:S(2)}, u32[]{:S(2)}) %collective-permute-start.9) | collective-permute-done | bytes 262176 | tf_op jit(solution)/shard_map/ppermute | solution.py:126
  165.7 9.7 %collective-permute-done.10 = bf16[256,512]{1,0:T(8,128)(2,1)S(1)} collective-permute-done((bf16[256,512]{1,0:T(8,128)(2,1)S(1)}, bf16[256,512]{1,0:T(8,128)(2,1)S(1)}, u32[]{:S(2)}, u32[]{:S(2)}) %collective-permute-start.10) | collective-permute-done | bytes 262176 | tf_op jit(solution)/shard_map/ppermute | solution.py:126
  176.5 9.6 %collective-permute-done.11 = bf16[256,512]{1,0:T(8,128)(2,1)} collective-permute-done((bf16[256,512]{1,0:T(8,128)(2,1)S(1)}, bf16[256,512]{1,0:T(8,128)(2,1)}, u32[]{:S(2)}, u32[]{:S(2)}) %collective-permute-start.11) | collective-permute-done | bytes 262176 | tf_op jit(solution)/shard_map/ppermute | solution.py:126
  186.7 9.7 %collective-permute-done.12 = bf16[256,512]{1,0:T(8,128)(2,1)} collective-permute-done((bf16[256,512]{1,0:T(8,128)(2,1)}, bf16[256,512]{1,0:T(8,128)(2,1)}, u32[]{:S(2)}, u32[]{:S(2)}) %collective-permute-start.12) | collective-permute-done | bytes 262176 | tf_op jit(solution)/shard_map/ppermute | solution.py:126
  196.9 9.7 %collective-permute-done.13 = bf16[256,512]{1,0:T(8,128)(2,1)S(1)} collective-permute-done((bf16[256,512]{1,0:T(8,128)(2,1)}, bf16[256,512]{1,0:T(8,128)(2,1)S(1)}, u32[]{:S(2)}, u32[]{:S(2)}) %collective-permute-start.13) | collective-permute-done | bytes 262176 | tf_op jit(solution)/shard_map/ppermute | solution.py:126
  209.4 7.5 %collective-permute-done.14 = bf16[256,512]{1,0:T(8,128)(2,1)S(1)} collective-permute-done((bf16[256,512]{1,0:T(8,128)(2,1)S(1)}, bf16[256,512]{1,0:T(8,128)(2,1)S(1)}, u32[]{:S(2)}, u32[]{:S(2)}) %collective-permute-start.14) | collective-permute-done | bytes 262176 | tf_op jit(solution)/shard_map/ppermute | solution.py:126
  220.3 6.6 %collective-permute-done.15 = bf16[256,512]{1,0:T(8,128)(2,1)S(1)} collective-permute-done((bf16[256,512]{1,0:T(8,128)(2,1)S(1)}, bf16[256,512]{1,0:T(8,128)(2,1)S(1)}, u32[]{:S(2)}, u32[]{:S(2)}) %collective-permute-start.15) | collective-permute-done | bytes 262176 | tf_op jit(solution)/shard_map/ppermute | solution.py:126
  237.7 11.2 %reshape.155 = bf16[2,8,256,8,64]{4,3,2,1,0:T(8,128)(2,1)} reshape(bf16[4096,512]{1,0:T(8,128)(2,1)} %constant_dynamic-slice_fusion.1) | data formatting | bytes 8388608 | tf_op jit(solution)/shard_map/reshape | solution.py:135
  248.9 9.7 %copy.43 = bf16[2,8,256,8,64]{2,4,1,3,0:T(8,128)(2,1)} copy(bf16[2,8,256,8,64]{4,3,2,1,0:T(8,128)(2,1)} %reshape.155) | data formatting | bytes 8388608
  258.6 11.2 %reshape.154 = bf16[2,8,256,8,64]{4,3,2,1,0:T(8,128)(2,1)} reshape(bf16[4096,512]{1,0:T(8,128)(2,1)} %all-gather.5.cloned.1.call-done) | data formatting | bytes 8388608 | tf_op jit(solution)/shard_map/reshape | solution.py:134
  269.9 9.8 %copy.41 = bf16[2,8,256,8,64]{2,4,1,3,0:T(8,128)(2,1)} copy(bf16[2,8,256,8,64]{4,3,2,1,0:T(8,128)(2,1)} %reshape.154) | data formatting | bytes 8388608
  279.7 46.1 %while.15 = (s32[]{:T(128)}, f32[256,8]{0,1:T(8,128)S(1)}, f32[256,8]{0,1:T(8,128)S(1)}, f32[256,8,64]{0,2,1:T(8,128)S(1)}, s32[2,8,256]{2,1,0:T(8,128)S(1)}, /*...) while((s32[]{:T(128)}, f32[256,8]{0,1:T(8,128)S(1)}, ...), condition=%wide.region_11.12_spmd.clone, body=%wide.region_5.11_spmd.clone.sunk | while | flops 1122789632 | bytes 127101120 | solution.py:138
  280.2 7.0 %fusion.69 = (f32[256,8,8]{0,2,1:T(8,128)S(1)}, f32[256,8,8,256]{0,3,2,1:T(8,128)S(1)}) fusion(f32[8,8,256]{2,1,0:T(8,128)S(1)} %bitcast.72, f32[256,8]{0,1:T(8,128)S(1)} %get-tuple-element.297, bf16[256,8,64]{0,2,1:T(8,128)(2,1)S(1)} %get-tuple-element.296, bf16[2,8,256,8,64]{2,4,1,3,0:T(8,128)(2,1)} %get-tuple-element.295, s32[]{:T(128)S(6)} %copy.93, ...), kind=kOutput, calls=%fused_computation.125.clone.1 | convolution fusion | flops 553631744 | bytes 19800068 | tf_op jit(solution)/shard_map/while/body/eval_jaxpr/qhd,gkhd->qhgk/dot_general | solution.py:25
  293.0 9.5 %fusion.72 = f32[256,8,64]{0,2,1:T(8,128)S(1)} fusion(f32[256,8,8,256]{0,3,2,1:T(8,128)} %copy-done.2, f32[256,8,8]{0,2,1:T(8,128)S(1)} %get-tuple-element.257, pred[256,8,256]{0,2,1:T(8,128)(4,1)S(1)} %broadcast_compare_fusion.6, bf16[2,8,256,8,64]{2,4,1,3,0:T(8,128)(2,1)} %get-tuple-element.299, s32[]{:T(128)S(6)} %copy.93, ...), kind=kOutput, calls=%fused_computation.12.clone.1 | convolution fusion | flops 551419904 | bytes 20054020 | tf_op jit(solution)/shard_map/while/body/eval_jaxpr/qhgk,gkhd->qhgd/dot_general | solution.py:32
  303.3 7.0 %fusion.69 = (f32[256,8,8]{0,2,1:T(8,128)S(1)}, f32[256,8,8,256]{0,3,2,1:T(8,128)S(1)}) fusion(f32[8,8,256]{2,1,0:T(8,128)S(1)} %bitcast.72, f32[256,8]{0,1:T(8,128)S(1)} %get-tuple-element.297, bf16[256,8,64]{0,2,1:T(8,128)(2,1)S(1)} %get-tuple-element.296, bf16[2,8,256,8,64]{2,4,1,3,0:T(8,128)(2,1)} %get-tuple-element.295, s32[]{:T(128)S(6)} %copy.93, ...), kind=kOutput, calls=%fused_computation.125.clone.1 | convolution fusion | flops 553631744 | bytes 19800068 | tf_op jit(solution)/shard_map/while/body/eval_jaxpr/qhd,gkhd->qhgk/dot_general | solution.py:25
  316.0 9.5 %fusion.72 = f32[256,8,64]{0,2,1:T(8,128)S(1)} fusion(f32[256,8,8,256]{0,3,2,1:T(8,128)} %copy-done.2, f32[256,8,8]{0,2,1:T(8,128)S(1)} %get-tuple-element.257, pred[256,8,256]{0,2,1:T(8,128)(4,1)S(1)} %broadcast_compare_fusion.6, bf16[2,8,256,8,64]{2,4,1,3,0:T(8,128)(2,1)} %get-tuple-element.299, s32[]{:T(128)S(6)} %copy.93, ...), kind=kOutput, calls=%fused_computation.12.clone.1 | convolution fusion | flops 551419904 | bytes 20054020 | tf_op jit(solution)/shard_map/while/body/eval_jaxpr/qhgk,gkhd->qhgd/dot_general | solution.py:32
  (177 shorter events, 64.7 us)
Async XLA Ops:
  6.5 144.3 %copy-start.28 = (f32[2048]{0:T(1024)S(1)}, f32[2048]{0:T(1024)}, u32[]{:S(2)}) copy-start(f32[2048]{0:T(1024)} %param.14) | copy-start | bytes 24580
  6.5 100.7 %copy-start.26 = (f32[256,8]{0,1:T(8,128)S(1)}, f32[256,8]{0,1:T(8,128)}, u32[]{:S(2)}) copy-start(f32[256,8]{0,1:T(8,128)} %param.21) | copy-start | bytes 24580
  6.5 14.1 %all-gather.3.cloned.1.call-start = ((), (), s32[]{:S(2)}) async-start(), calls=%async_computation | async-start | bytes 1572864 | tf_op jit(solution)/shard_map/all_gather | solution.py:73
  7.3 251.4 %all-gather.5.cloned.1.call-start = ((), (), s32[]{:S(2)}) async-start(), calls=%async_computation.1 | async-start | bytes 4456448 | tf_op jit(solution)/shard_map/all_gather | solution.py:121
  25.6 12.2 %collective-permute-start.1 = (bf16[256,512]{1,0:T(8,128)(2,1)S(1)}, bf16[256,512]{1,0:T(8,128)(2,1)S(1)}, u32[]{:S(2)}, u32[]{:S(2)}) collective-permute-start(bf16[256,512]{1,0:T(8,128)(2,1)S(1)} %convolution_convert_fusion), channel_id=1, source_target_pairs={{0,2},{2,4},{4,6},{6,8},{8,10},{10,12},{12,14},{14,16},{16,18},{18... | collective-permute-start | bytes 786440 | tf_op jit(solution)/shard_map/ppermute | solution.py:126
  38.5 11.3 %collective-permute-start.2 = (bf16[256,512]{1,0:T(8,128)(2,1)S(1)}, bf16[256,512]{1,0:T(8,128)(2,1)S(1)}, u32[]{:S(2)}, u32[]{:S(2)}) collective-permute-start(bf16[256,512]{1,0:T(8,128)(2,1)S(1)} %collective-permute-done.1), channel_id=1, source_target_pairs={{0,2},{2,4},{4,6},{6,8},{8,10},{10,12},{12,14},{14,16},{16,18},{18... | collective-permute-start | bytes 786440 | tf_op jit(solution)/shard_map/ppermute | solution.py:126
  49.8 10.5 %collective-permute-start.3 = (bf16[256,512]{1,0:T(8,128)(2,1)S(1)}, bf16[256,512]{1,0:T(8,128)(2,1)S(1)}, u32[]{:S(2)}, u32[]{:S(2)}) collective-permute-start(bf16[256,512]{1,0:T(8,128)(2,1)S(1)} %collective-permute-done.2), channel_id=1, source_target_pairs={{0,2},{2,4},{4,6},{6,8},{8,10},{10,12},{12,14},{14,16},{16,18},{18... | collective-permute-start | bytes 786440 | tf_op jit(solution)/shard_map/ppermute | solution.py:126
  60.3 10.0 %collective-permute-start.4 = (bf16[256,512]{1,0:T(8,128)(2,1)S(1)}, bf16[256,512]{1,0:T(8,128)(2,1)S(1)}, u32[]{:S(2)}, u32[]{:S(2)}) collective-permute-start(bf16[256,512]{1,0:T(8,128)(2,1)S(1)} %collective-permute-done.3), channel_id=1, source_target_pairs={{0,2},{2,4},{4,6},{6,8},{8,10},{10,12},{12,14},{14,16},{16,18},{18... | collective-permute-start | bytes 786440 | tf_op jit(solution)/shard_map/ppermute | solution.py:126
  63.2 112.2 %copy-start.27 = (f32[64]{0:T(128)S(1)}, f32[64]{0:T(128)}, u32[]{:S(2)}) copy-start(f32[64]{0:T(128)} %param.19) | copy-start | bytes 772
  70.2 106.0 %copy-start.11 = (bf16[256,512]{1,0:T(8,128)(2,1)}, bf16[256,512]{1,0:T(8,128)(2,1)S(1)}, u32[]{:S(2)}) copy-start(bf16[256,512]{1,0:T(8,128)(2,1)S(1)} %collective-permute-done.4) | copy-start | bytes 786436
  70.2 10.0 %collective-permute-start.5 = (bf16[256,512]{1,0:T(8,128)(2,1)S(1)}, bf16[256,512]{1,0:T(8,128)(2,1)S(1)}, u32[]{:S(2)}, u32[]{:S(2)}) collective-permute-start(bf16[256,512]{1,0:T(8,128)(2,1)S(1)} %collective-permute-done.4), channel_id=1, source_target_pairs={{0,2},{2,4},{4,6},{6,8},{8,10},{10,12},{12,14},{14,16},{16,18},{18... | collective-permute-start | bytes 786440 | tf_op jit(solution)/shard_map/ppermute | solution.py:126
  80.2 96.2 %copy-start.13 = (bf16[256,512]{1,0:T(8,128)(2,1)}, bf16[256,512]{1,0:T(8,128)(2,1)S(1)}, u32[]{:S(2)}) copy-start(bf16[256,512]{1,0:T(8,128)(2,1)S(1)} %collective-permute-done.5) | copy-start | bytes 786436
  80.2 10.1 %collective-permute-start.6 = (bf16[256,512]{1,0:T(8,128)(2,1)S(1)}, bf16[256,512]{1,0:T(8,128)(2,1)S(1)}, u32[]{:S(2)}, u32[]{:S(2)}) collective-permute-start(bf16[256,512]{1,0:T(8,128)(2,1)S(1)} %collective-permute-done.5), channel_id=1, source_target_pairs={{0,2},{2,4},{4,6},{6,8},{8,10},{10,12},{12,14},{14,16},{16,18},{18... | collective-permute-start | bytes 786440 | tf_op jit(solution)/shard_map/ppermute | solution.py:126
  90.3 86.0 %copy-start.15 = (bf16[256,512]{1,0:T(8,128)(2,1)}, bf16[256,512]{1,0:T(8,128)(2,1)S(1)}, u32[]{:S(2)}) copy-start(bf16[256,512]{1,0:T(8,128)(2,1)S(1)} %collective-permute-done.6) | copy-start | bytes 786436
  90.3 16.9 %collective-permute-start.7 = (bf16[256,512]{1,0:T(8,128)(2,1)S(1)}, bf16[256,512]{1,0:T(8,128)(2,1)S(1)}, u32[]{:S(2)}, u32[]{:S(2)}) collective-permute-start(bf16[256,512]{1,0:T(8,128)(2,1)S(1)} %collective-permute-done.6), channel_id=1, source_target_pairs={{0,2},{2,4},{4,6},{6,8},{8,10},{10,12},{12,14},{14,16},{16,18},{18... | collective-permute-start | bytes 786440 | tf_op jit(solution)/shard_map/ppermute | solution.py:126
  107.2 43.6 %collective-permute-start.8 = (bf16[256,512]{1,0:T(8,128)(2,1)S(1)}, bf16[256,512]{1,0:T(8,128)(2,1)S(1)}, u32[]{:S(2)}, u32[]{:S(2)}) collective-permute-start(bf16[256,512]{1,0:T(8,128)(2,1)S(1)} %collective-permute-done.7), channel_id=1, source_target_pairs={{0,2},{2,4},{4,6},{6,8},{8,10},{10,12},{12,14},{14,16},{16,18},{18... | collective-permute-start | bytes 786440 | tf_op jit(solution)/shard_map/ppermute | solution.py:126
  150.8 12.0 %collective-permute-start.9 = (bf16[256,512]{1,0:T(8,128)(2,1)S(1)}, bf16[256,512]{1,0:T(8,128)(2,1)S(1)}, u32[]{:S(2)}, u32[]{:S(2)}) collective-permute-start(bf16[256,512]{1,0:T(8,128)(2,1)S(1)} %collective-permute-done.8), channel_id=1, source_target_pairs={{0,2},{2,4},{4,6},{6,8},{8,10},{10,12},{12,14},{14,16},{16,18},{18... | collective-permute-start | bytes 786440 | tf_op jit(solution)/shard_map/ppermute | solution.py:126
  153.6 22.7 %collective-permute-start = (bf16[16,512]{1,0:T(8,128)(2,1)S(1)}, bf16[16,512]{1,0:T(8,128)(2,1)S(1)}, u32[]{:S(2)}, u32[]{:S(2)}) collective-permute-start(bf16[16,512]{1,0:T(8,128)(2,1)S(1)} %slice.42), channel_id=1, source_target_pairs={{0,2},{2,4},{4,6},{6,8},{8,10},{10,12},{12,14},{14,16},{16,18},{18... | collective-permute-start | bytes 49160 | tf_op jit(solution)/shard_map/ppermute | solution.py:17
  162.8 12.6 %collective-permute-start.10 = (bf16[256,512]{1,0:T(8,128)(2,1)S(1)}, bf16[256,512]{1,0:T(8,128)(2,1)S(1)}, u32[]{:S(2)}, u32[]{:S(2)}) collective-permute-start(bf16[256,512]{1,0:T(8,128)(2,1)S(1)} %collective-permute-done.9), channel_id=1, source_target_pairs={{0,2},{2,4},{4,6},{6,8},{8,10},{10,12},{12,14},{14,16},{16,18},{18... | collective-permute-start | bytes 786440 | tf_op jit(solution)/shard_map/ppermute | solution.py:126
  175.4 10.7 %collective-permute-start.11 = (bf16[256,512]{1,0:T(8,128)(2,1)S(1)}, bf16[256,512]{1,0:T(8,128)(2,1)}, u32[]{:S(2)}, u32[]{:S(2)}) collective-permute-start(bf16[256,512]{1,0:T(8,128)(2,1)S(1)} %collective-permute-done.10), channel_id=1, source_target_pairs={{0,2},{2,4},{4,6},{6,8},{8,10},{10,12},{12,14},{14,16},{16,18},{18... | collective-permute-start | bytes 786440 | tf_op jit(solution)/shard_map/ppermute | solution.py:126
  186.1 10.3 %collective-permute-start.12 = (bf16[256,512]{1,0:T(8,128)(2,1)}, bf16[256,512]{1,0:T(8,128)(2,1)}, u32[]{:S(2)}, u32[]{:S(2)}) collective-permute-start(bf16[256,512]{1,0:T(8,128)(2,1)} %collective-permute-done.11), channel_id=1, source_target_pairs={{0,2},{2,4},{4,6},{6,8},{8,10},{10,12},{12,14},{14,16},{16,18},{18... | collective-permute-start | bytes 786440 | tf_op jit(solution)/shard_map/ppermute | solution.py:126
  196.4 10.2 %collective-permute-start.13 = (bf16[256,512]{1,0:T(8,128)(2,1)}, bf16[256,512]{1,0:T(8,128)(2,1)S(1)}, u32[]{:S(2)}, u32[]{:S(2)}) collective-permute-start(bf16[256,512]{1,0:T(8,128)(2,1)} %collective-permute-done.12), channel_id=1, source_target_pairs={{0,2},{2,4},{4,6},{6,8},{8,10},{10,12},{12,14},{14,16},{16,18},{18... | collective-permute-start | bytes 786440 | tf_op jit(solution)/shard_map/ppermute | solution.py:126
  206.6 10.4 %collective-permute-start.14 = (bf16[256,512]{1,0:T(8,128)(2,1)S(1)}, bf16[256,512]{1,0:T(8,128)(2,1)S(1)}, u32[]{:S(2)}, u32[]{:S(2)}) collective-permute-start(bf16[256,512]{1,0:T(8,128)(2,1)S(1)} %collective-permute-done.13), channel_id=1, source_target_pairs={{0,2},{2,4},{4,6},{6,8},{8,10},{10,12},{12,14},{14,16},{16,18},{18... | collective-permute-start | bytes 786440 | tf_op jit(solution)/shard_map/ppermute | solution.py:126
  216.9 10.0 %collective-permute-start.15 = (bf16[256,512]{1,0:T(8,128)(2,1)S(1)}, bf16[256,512]{1,0:T(8,128)(2,1)S(1)}, u32[]{:S(2)}, u32[]{:S(2)}) collective-permute-start(bf16[256,512]{1,0:T(8,128)(2,1)S(1)} %collective-permute-done.14), channel_id=1, source_target_pairs={{0,2},{2,4},{4,6},{6,8},{8,10},{10,12},{12,14},{14,16},{16,18},{18... | collective-permute-start | bytes 786440 | tf_op jit(solution)/shard_map/ppermute | solution.py:126
  (24 other events, 652.7 us)
Sparse Core Ops, SparseCore 0:
  8.9 11.7 all-gather.2
  81.2 89.1 all-gather.4
